TPU v7x, 32 devices: a whole 2x2x4 slice. The times are simulated.
32 devices in a mesh: sp: 4 (over z), fs: 4 (over y, x), tp: 2 (over core).
Axes of the slice: x: 2, y: 2, z: 4, core: 2. Of those that a mesh axis runs over, the one named last changes fastest.
Arguments:
- inputs: bfloat16 [4, 1024, 4096], P('fs', 'sp', 'tp'), may hold values from -6 to 6
- norm_gain: float32 [4096], replicated, may hold values from 0.1 to 1.9
- conv_in_a: bfloat16 [4096, 1024], P(('sp', 'fs'), 'tp'), may hold values from -0.09375 to 0.09375
- conv_in_b: bfloat16 [4096, 1024], P(('sp', 'fs'), 'tp'), may hold values from -0.09375 to 0.09375
- query_w: bfloat16 [4096, 512], P(('sp', 'fs'), 'tp'), may hold values from -0.09375 to 0.09375
- key_w: bfloat16 [4096, 512], P(('sp', 'fs'), 'tp'), may hold values from -0.09375 to 0.09375
- value_w: bfloat16 [4096, 1024], P(('sp', 'fs'), 'tp'), may hold values from -0.09375 to 0.09375
- out_gate_w: bfloat16 [4096, 1024], P(('sp', 'fs'), 'tp'), may hold values from -0.09375 to 0.09375
- pointwise_w: bfloat16 [4096, 1024], P(('sp', 'fs'), 'tp'), may hold values from -0.1875 to 0.1875
- gla_out_w: bfloat16 [4096, 1024], P(('sp', 'fs'), 'tp'), may hold values from -0.1875 to 0.1875
- forget_first_factor: bfloat16 [4096, 64], replicated, may hold values from -0.09375 to 0.09375
- decay_w: bfloat16 [64, 512], replicated, may hold values from -0.75 to 0.75
- decay_bias: float32 [512], replicated, as said below
- decay_extra: float32 [4, 1024, 512], P('fs', 'sp', 'tp'), may hold values from -2.2 to 0, as said below
- conv_kernel: float32 [31, 1024], replicated, may hold values from -7 to 7
- conv_gain: float32 [1024], replicated, may hold values from 0.1 to 1.9
- head_gain: float32 [64], replicated, may hold values from 0.1 to 1.9
Outputs:
- mixed: bfloat16 [4, 1024, 4096], P('fs', 'sp', 'tp')
Inputs may be any that keep to these rules, and one draw needn't show every extreme that they name: decay_bias is positive. decay_extra is never positive.
All inputs are finite; a program needn't handle non-finite values.
Results may differ from a plain program's by a relative error of at most 0.015.
Values may be sent and summed in bfloat16 or wider, within the bound.
A program may use at most 192 MiB of HBM per device.

v0:
```python
import jax
import jax.numpy as jnp
from jax import lax
from jax.sharding import PartitionSpec as P

DK = 32
DV = 64
BLOCK = 64


def from_behind(value, axis, by):
    length = lax.axis_size(axis)
    pairs = [(i, i + by) for i in range(length) if 0 <= i + by < length]
    return lax.ppermute(value, axis, pairs)


def shards(
    inputs,
    norm_gain,
    conv_in_a,
    conv_in_b,
    query_w,
    key_w,
    value_w,
    out_gate_w,
    pointwise_w,
    gla_out_w,
    forget_first_factor,
    decay_w,
    decay_bias,
    decay_extra,
    conv_kernel,
    conv_gain,
    head_gain,
):
    collected = (
        lax.all_gather(conv_in_a, ("sp", "fs"), axis=0, tiled=True),
        lax.all_gather(conv_in_b, ("sp", "fs"), axis=0, tiled=True),
        lax.all_gather(query_w, ("sp", "fs"), axis=0, tiled=True),
        lax.all_gather(key_w, ("sp", "fs"), axis=0, tiled=True),
        lax.all_gather(value_w, ("sp", "fs"), axis=0, tiled=True),
        lax.all_gather(out_gate_w, ("sp", "fs"), axis=0, tiled=True),
        lax.all_gather(pointwise_w, ("sp", "fs"), axis=0, tiled=True),
        lax.all_gather(gla_out_w, ("sp", "fs"), axis=0, tiled=True),
    )
    (
        conv_a_full,
        conv_b_full,
        query_full,
        key_full,
        value_full,
        gate_full,
        pointwise_full,
        gla_out_full,
    ) = collected
    tok_rows = inputs[0]
    token_count = tok_rows.shape[0]
    in_weights = (
        conv_a_full,
        conv_b_full,
        query_full,
        key_full,
        value_full,
        gate_full,
        forget_first_factor,
    )
    segment_values = lax.all_gather(tok_rows, "tp", axis=1, tiled=True).astype(jnp.float32)
    scaled = (segment_values * norm_gain).astype(jnp.bfloat16)
    sums = tuple(
        (jnp.dot(scaled, weight, preferred_element_type=jnp.float32) for weight in in_weights)
    )
    sums, squares = (sums, jnp.sum(segment_values * segment_values, axis=1))
    row_scale = lax.rsqrt(squares / norm_gain.shape[0] + 1e-06)[:, None]
    conv_a, conv_b, queries, keys, values, out_gate, low_rank = [
        (running * row_scale).astype(jnp.bfloat16) for running in sums
    ]
    gated = (conv_a.astype(jnp.float32) * jax.nn.sigmoid(conv_b.astype(jnp.float32))).astype(
        jnp.bfloat16
    )
    reach = conv_kernel.shape[0] - 1
    earlier = from_behind(gated[token_count - reach :], "sp", 1)
    extended = jnp.concatenate([earlier, gated], axis=0).astype(jnp.float32)
    tp_index = lax.axis_index("tp")
    channels = gated.shape[1]
    kernel = lax.dynamic_slice_in_dim(conv_kernel, tp_index * channels, channels, 1)
    convolved = jnp.zeros((token_count, channels), jnp.float32)
    for offset in range(reach + 1):
        convolved = convolved + kernel[offset] * extended[offset : offset + token_count]
    channel_sum, channel_squares = lax.psum(
        (jnp.sum(convolved, axis=1), jnp.sum(convolved * convolved, axis=1)), "tp"
    )
    total_channels = conv_gain.shape[0]
    average = channel_sum / total_channels
    spread_squared_mean = channel_squares / total_channels - average * average
    gain_part = lax.dynamic_slice_in_dim(conv_gain, tp_index * channels, channels)
    normed = (
        (convolved - average[:, None]) * lax.rsqrt(spread_squared_mean + 1e-05)[:, None] * gain_part
    )
    conv_act = jax.nn.silu(normed).astype(jnp.bfloat16)
    key_width = keys.shape[1]
    head_count = key_width // DK
    decay_part = lax.dynamic_slice_in_dim(decay_w, tp_index * key_width, key_width, 1)
    bias_part = lax.dynamic_slice_in_dim(decay_bias, tp_index * key_width, key_width)
    pre_decay = jnp.dot(low_rank, decay_part, preferred_element_type=jnp.float32) + bias_part
    log_decay = jax.nn.log_sigmoid(pre_decay) / 16.0 + decay_extra[0]
    block_count = token_count // BLOCK
    highest = lax.Precision.HIGHEST

    def split_blocks(array_operand, width):
        return array_operand.reshape(block_count, BLOCK, head_count, width).transpose(0, 2, 1, 3)

    q_blocks = split_blocks(queries.astype(jnp.float32), DK) * DK ** (-0.5)
    k_blocks = split_blocks(keys.astype(jnp.float32), DK)
    v_blocks = split_blocks(values.astype(jnp.float32), DV)
    prefix_running_sum = jnp.cumsum(split_blocks(log_decay, DK), axis=2)
    causal = jnp.tril(jnp.ones((BLOCK, BLOCK), dtype=bool))
    spread = prefix_running_sum[:, :, :, None, :] - prefix_running_sum[:, :, None, :, :]
    weights_in = jnp.exp(jnp.where(causal[:, :, None], spread, -jnp.inf))
    scores = jnp.einsum("nhid,nhjd,nhijd->nhij", q_blocks, k_blocks, weights_in, precision=highest)
    inner = jnp.einsum("nhij,nhjv->nhiv", scores, v_blocks, precision=highest)
    block_total = prefix_running_sum[:, :, -1]
    block_state = jnp.einsum(
        "nhjd,nhjv->nhdv",
        k_blocks * jnp.exp(block_total[:, :, None] - prefix_running_sum),
        v_blocks,
        precision=highest,
    )

    def advance(state, block_pair):
        decay_row, added_share_term = block_pair
        return (jnp.exp(decay_row)[..., None] * state + added_share_term, state)

    local_final, local_entering = lax.scan(
        advance, jnp.zeros((head_count, DK, DV), jnp.float32), (block_total, block_state)
    )
    device_total = jnp.sum(block_total, axis=0)
    totals = lax.all_gather(device_total[None], "sp", axis=0, tiled=True)
    running_totals = jnp.cumsum(totals, axis=0)
    sp_index = lax.axis_index("sp")
    before = lax.dynamic_index_in_dim(
        running_totals, sp_index, 0, False
    ) - lax.dynamic_index_in_dim(totals, sp_index, 0, False)
    piece = lax.all_gather(local_final[None], "sp", axis=0, tiled=True)
    number = piece.shape[0]
    anchor = jnp.arange(number, dtype=jnp.int32)
    exponent = jnp.where(
        (anchor < sp_index)[:, None, None], before[None] - running_totals, -jnp.inf
    )
    entering = jnp.einsum("nhd,nhdv->hdv", jnp.exp(exponent), piece, precision=highest)
    passed = jnp.exp(jnp.cumsum(block_total, axis=0) - block_total)
    entering_blocks = passed[..., None] * entering[None] + local_entering
    outer = jnp.einsum(
        "nhid,nhdv->nhiv",
        q_blocks * jnp.exp(prefix_running_sum),
        entering_blocks,
        precision=highest,
    )
    head_output = inner + outer
    normed_heads = (
        head_output
        * lax.rsqrt(jnp.mean(head_output * head_output, axis=-1, keepdims=True) + 1e-06)
        * head_gain
    )
    gla_rows = normed_heads.transpose(0, 2, 1, 3).reshape(token_count, head_count * DV)
    gla_act = (gla_rows * jax.nn.silu(out_gate.astype(jnp.float32))).astype(jnp.bfloat16)
    contract = (((1,), (1,)), ((), ()))
    conv_term = lax.dot_general(
        pointwise_full, conv_act, contract, preferred_element_type=jnp.float32
    )
    summed = lax.psum_scatter(
        (
            conv_term
            + lax.dot_general(gla_out_full, gla_act, contract, preferred_element_type=jnp.float32)
        ).astype(jnp.bfloat16),
        "tp",
        scatter_dimension=0,
        tiled=True,
    ).astype(jnp.float32)
    return (tok_rows.astype(jnp.float32) + summed.T).astype(jnp.bfloat16)[None]


def solution(mesh):
    return jax.shard_map(
        shards,
        mesh=mesh,
        in_specs=(
            P("fs", "sp", "tp"),
            P(),
            P(("sp", "fs"), "tp"),
            P(("sp", "fs"), "tp"),
            P(("sp", "fs"), "tp"),
            P(("sp", "fs"), "tp"),
            P(("sp", "fs"), "tp"),
            P(("sp", "fs"), "tp"),
            P(("sp", "fs"), "tp"),
            P(("sp", "fs"), "tp"),
            P(),
            P(),
            P(),
            P("fs", "sp", "tp"),
            P(),
            P(),
            P(),
        ),
        out_specs=P("fs", "sp", "tp"),
        check_vma=False,
    )
```

profile of v0, /device:TPU:0, one launch (start us, length us, event | category | flops | bytes accessed | tf_op | source)
XLA Modules:
  0.0 639.4 jit_solution(9159292543313479262)
XLA Ops:
  6.6 0.7 all-gather.29.cloned.1.call-update
  7.3 0.7 all-gather.21.cloned.1.call-update
  8.1 0.7 all-gather.19.cloned.1.call-update
  8.8 0.5 all-gather.23.cloned.1.call-update
  9.4 0.5 all-gather.15.cloned.1.call-update
  10.0 0.5 all-gather.13.cloned.1.call-update
  10.5 0.7 all-gather.17.cloned.1.call-update
  11.3 0.7 all-gather.25.cloned.1.call-update
  12.0 0.7 all-gather.27.cloned.1.call-update
  12.8 0.8 dynamic_slice.30
  13.6 1.4 dynamic_slice.28
  15.0 1.8 fusion.105
  16.8 2.0 constant_dynamic-slice_fusion
  18.8 3.4 all-gather.29.cloned.1.call-done
  22.2 2.1 fusion.4
  24.4 2.8 fusion.85
  27.3 0.2 reshape.63
  27.5 0.4 copy.58
  27.9 25.9 %fusion.106 = f32[4,8,64,32]{3,1,2,0:T(8,128)S(1)} fusion(f32[4,8,64,32]{3,1,2,0:T(8,128)S(1)} %copy.58), kind=kOutput, calls=%fused_computation.161 | output fusion | flops 4128768 | bytes 524288 | tf_op jit(solution)/shard_map/jit(cumsum)/reduce_window_sum | solution.py:115
  54.0 0.3 copy.60
  54.4 0.6 fusion.26
  55.0 13.7 %all-gather.1 = f32[32,32]{1,0:T(8,128)S(1)} all-gather(f32[8,32]{1,0:T(8,128)S(1)} %get-tuple-element.68), channel_id=3, replica_groups=mesh['sp'=4,'fs'=4,'tp'=2] {'sp'}, dimensions={0}, use_global_device_ids=true | all-gather | bytes 5120 | tf_op jit(solution)/shard_map/all_gather | solution.py:137
  68.9 0.8 copy.80
  69.7 11.5 %select_exponential_fusion = f32[4,8,64,64,32]{3,4,2,1,0:T(8,128)} fusion(f32[4,8,64,32]{2,3,1,0:T(8,128)S(1)} %copy.60, f32[4,8,64,32]{3,2,1,0:T(8,128)S(1)} %copy.59, pred[64,64]{1,0:T(8,128)(4,1)S(1)} %iota_compare_fusion), kind=kLoop, calls=%fused_computation.5 | loop fusion | flops 8388608 | bytes 17305600 | tf_op jit(solution)/shard_map/exp | solution.py:118
  81.2 35.4 %copy.76 = f32[4,8,64,64,32]{2,3,4,1,0:T(8,128)} copy(f32[4,8,64,64,32]{3,4,2,1,0:T(8,128)} %select_exponential_fusion) | data formatting | bytes 33554432
  116.6 3.0 fusion.24
  119.9 28.6 %all-gather.19.cloned.1.call-done = bf16[4096,256]{1,0:T(8,128)(2,1)} async-done(((bf16[256,256]{1,0:T(8,128)(2,1)}), bf16[4096,256]{1,0:T(8,128)(2,1)}) %all-gather.19.cloned.1.call-update) | async-done | bytes 2097168 | tf_op jit(solution)/shard_map/all_gather | solution.py:40
  148.6 2.9 fusion.21
  152.0 12.0 %fusion = f32[4,8,64,64]{2,3,1,0:T(8,128)S(1)} fusion(f32[4,8,64,64,32]{2,3,4,1,0:T(8,128)} %copy.76, f32[4,8,32,64]{3,2,1,0:T(8,128)S(1)} %copy.64, f32[4,8,32,64]{3,2,1,0:T(8,128)S(1)} %copy.62), kind=kLoop, calls=%fused_computation.4 | loop fusion | flops 12451840 | bytes 17825792 | tf_op jit(solution)/shard_map/nhid,nhjd,nhijd->nhij/dot_general | solution.py:119
  164.0 1.4 copy.67
  165.4 1.3 copy.68
  166.7 3.2 bitcast_multiply_fusion.2
  169.9 55.8 %all-gather.23.cloned.1.call-done = bf16[4096,512]{1,0:T(8,128)(2,1)} async-done(((bf16[256,512]{1,0:T(8,128)(2,1)}), bf16[4096,512]{1,0:T(8,128)(2,1)}) %all-gather.23.cloned.1.call-update) | async-done | bytes 4194320 | tf_op jit(solution)/shard_map/all_gather | solution.py:41
  225.6 4.1 fusion.16
  229.7 0.3 reshape.65
  230.0 72.5 %all-gather.15.cloned.1.call-done = bf16[4096,512]{1,0:T(8,128)(2,1)} async-done(((bf16[256,512]{1,0:T(8,128)(2,1)}), bf16[4096,512]{1,0:T(8,128)(2,1)}) %all-gather.15.cloned.1.call-update) | async-done | bytes 4194320 | tf_op jit(solution)/shard_map/all_gather | solution.py:38
  302.5 5.0 fusion.15
  307.4 71.9 %all-gather.13.cloned.1.call-done = bf16[4096,512]{1,0:T(8,128)(2,1)} async-done(((bf16[256,512]{1,0:T(8,128)(2,1)}), bf16[4096,512]{1,0:T(8,128)(2,1)}) %all-gather.13.cloned.1.call-update) | async-done | bytes 4194320 | tf_op jit(solution)/shard_map/all_gather | solution.py:37
  379.3 4.2 fusion.9
  383.5 0.6 slice.256
  384.1 4.0 collective-permute-start
  388.1 1.0 fusion.30
  389.1 3.3 while.13
  389.1 0.7 bitcast_dynamic-update-slice_fusion.2
  389.9 0.7 bitcast_dynamic-update-slice_fusion.2
  390.7 0.7 bitcast_dynamic-update-slice_fusion.2
  391.6 0.7 bitcast_dynamic-update-slice_fusion.2
  392.4 18.4 %all-gather.2 = f32[32,32,64]{2,1,0:T(8,128)S(1)} all-gather(f32[8,32,64]{2,1,0:T(8,128)S(1)} %get-tuple-element.33), channel_id=4, replica_groups=mesh['sp'=4,'fs'=4,'tp'=2] {'sp'}, dimensions={0}, use_global_device_ids=true | all-gather | bytes 327680 | tf_op jit(solution)/shard_map/all_gather | solution.py:143
  410.8 2.9 fusion.80
  413.8 0.8 fusion.70
  414.6 2.1 multiply_reduce_fusion
  417.0 0.3 fusion.28
  417.3 0.4 copy.71
  417.7 0.3 reshape.66
  418.0 0.8 maximum_convert_fusion
  419.1 2.6 fusion.103
  421.8 2.5 all-reduce
  424.3 34.2 %all-gather.17.cloned.1.call-done = bf16[4096,512]{1,0:T(8,128)(2,1)} async-done(((bf16[256,512]{1,0:T(8,128)(2,1)}), bf16[4096,512]{1,0:T(8,128)(2,1)}) %all-gather.17.cloned.1.call-update) | async-done | bytes 4194320 | tf_op jit(solution)/shard_map/all_gather | solution.py:43
  458.4 5.6 fusion.82
  464.0 71.4 %all-gather.25.cloned.1.call-done = bf16[4096,512]{1,0:T(8,128)(2,1)} async-done(((bf16[256,512]{1,0:T(8,128)(2,1)}), bf16[4096,512]{1,0:T(8,128)(2,1)}) %all-gather.25.cloned.1.call-update) | async-done | bytes 4194320 | tf_op jit(solution)/shard_map/all_gather | solution.py:42
  535.4 77.0 %all-gather.27.cloned.1.call-done = bf16[4096,512]{1,0:T(8,128)(2,1)} async-done(((bf16[256,512]{1,0:T(8,128)(2,1)}), bf16[4096,512]{1,0:T(8,128)(2,1)}) %all-gather.27.cloned.1.call-update) | async-done | bytes 4194320 | tf_op jit(solution)/shard_map/all_gather | solution.py:44
  612.4 9.1 %fusion.2 = bf16[4096,256]{0,1:T(8,128)(2,1)} fusion(f32[256,4096]{1,0:T(8,128)} %fusion.82, bf16[4096,512]{1,0:T(8,128)(2,1)} %all-gather.27.cloned.1.call-done, f32[256,512]{1,0:T(8,128)S(1)} %reshape.66, bf16[4096,512]{1,0:T(8,128)(2,1)} %all-gather.25.cloned.1.call-done, bf16[1,256,4096]{2,1,0:T(8,128)(2,1)} %all-gather.29.cloned.1.call-done, ...), kind=kOutput, calls=%fused_computation.10 | convolution fusion | flops 2153906176 | bytes 17318912 | tf_op jit(solution)/shard_map/dot_general | solution.py:173
  621.6 8.4 %reduce-scatter.2.cloned.1.call-done = bf16[2048,256]{0,1:T(8,128)(2,1)} async-done(((bf16[4096,256]{0,1:T(8,128)(2,1)}), bf16[2048,256]{0,1:T(8,128)(2,1)}) %reduce-scatter.2.cloned.1.call-update) | async-done | bytes 1048592 | tf_op jit(solution)/shard_map/reduce_scatter | solution.py:170
  630.0 2.6 fusion.27
  (134 shorter events, 2.5 us)
Async XLA Ops:
  6.5 17.8 %copy-start = (bf16[4096,64]{0,1:T(8,128)(2,1)S(1)}, bf16[4096,64]{0,1:T(8,128)(2,1)}, u32[]{:S(2)}) copy-start(bf16[4096,64]{0,1:T(8,128)(2,1)} %param.29) | copy-start | bytes 1572868
  6.5 17.8 %copy-start.44 = (f32[4096]{0:T(1024)S(1)}, f32[4096]{0:T(1024)}, u32[]{:S(2)}) copy-start(f32[4096]{0:T(1024)} %param.20) | copy-start | bytes 49156
  6.5 17.8 %copy-start.43 = (bf16[64,512]{1,0:T(8,128)(2,1)S(1)}, bf16[64,512]{1,0:T(8,128)(2,1)}, u32[]{:S(2)}) copy-start(bf16[64,512]{1,0:T(8,128)(2,1)} %param.30) | copy-start | bytes 196612
  6.5 17.8 %copy-start.42 = (f32[1,256,256]{2,1,0:T(8,128)S(1)}, f32[1,256,256]{2,1,0:T(8,128)}, u32[]{:S(2)}) copy-start(f32[1,256,256]{2,1,0:T(8,128)} %param.32) | copy-start | bytes 786436
  6.5 15.7 %all-gather.29.cloned.1.call-start = ((), (), s32[]{:S(2)}) async-start(), calls=%async_computation.10 | async-start | bytes 3145728 | tf_op jit(solution)/shard_map/all_gather | solution.py:67
  7.3 109.3 %all-gather.21.cloned.1.call-start = ((), (), s32[]{:S(2)}) async-start(), calls=%async_computation.5 | async-start | bytes 2228224 | tf_op jit(solution)/shard_map/all_gather | solution.py:39
  8.0 140.6 %all-gather.19.cloned.1.call-start = ((), (), s32[]{:S(2)}) async-start(), calls=%async_computation.4 | async-start | bytes 2228224 | tf_op jit(solution)/shard_map/all_gather | solution.py:40
  8.8 216.9 %all-gather.23.cloned.1.call-start = ((), (), s32[]{:S(2)}) async-start(), calls=%async_computation.6 | async-start | bytes 4456448 | tf_op jit(solution)/shard_map/all_gather | solution.py:41
  9.3 293.1 %all-gather.15.cloned.1.call-start = ((), (), s32[]{:S(2)}) async-start(), calls=%async_computation.2 | async-start | bytes 4456448 | tf_op jit(solution)/shard_map/all_gather | solution.py:38
  9.9 369.4 %all-gather.13.cloned.1.call-start = ((), (), s32[]{:S(2)}) async-start(), calls=%async_computation.1 | async-start | bytes 4456448 | tf_op jit(solution)/shard_map/all_gather | solution.py:37
  10.5 447.9 %all-gather.17.cloned.1.call-start = ((), (), s32[]{:S(2)}) async-start(), calls=%async_computation.3 | async-start | bytes 4456448 | tf_op jit(solution)/shard_map/all_gather | solution.py:43
  11.2 524.2 %all-gather.25.cloned.1.call-start = ((), (), s32[]{:S(2)}) async-start(), calls=%async_computation.7 | async-start | bytes 4456448 | tf_op jit(solution)/shard_map/all_gather | solution.py:42
  12.0 600.4 %all-gather.27.cloned.1.call-start = ((), (), s32[]{:S(2)}) async-start(), calls=%async_computation.8 | async-start | bytes 4456448 | tf_op jit(solution)/shard_map/all_gather | solution.py:44
  12.7 617.2 %reduce-scatter.2.cloned.1.call-start = ((), (), s32[]{:S(2)}) async-start(), calls=%async_computation.9 | async-start | bytes 3145728 | tf_op jit(solution)/shard_map/reduce_scatter | solution.py:170
  24.4 278.1 %copy-start.39 = (f32[256]{0:T(256)}, f32[256]{0:T(256)S(1)}, u32[]{:S(2)}) copy-start(f32[256]{0:T(256)S(1)} %add_rsqrt_fusion.1) | copy-start | bytes 3076
  230.0 149.3 %copy-start.45 = (f32[4096]{0:T(1024)S(1)}, f32[4096]{0:T(1024)}, u32[]{:S(2)}) copy-start(f32[4096]{0:T(1024)} %param.20) | copy-start | bytes 49156
  307.4 80.7 %copy-start.3 = (f32[4,8,64,32]{3,1,2,0:T(8,128)S(1)}, f32[4,8,64,32]{3,1,2,0:T(8,128)}, u32[]{:S(2)}) copy-start(f32[4,8,64,32]{3,1,2,0:T(8,128)} %get-tuple-element.70) | copy-start | bytes 786436
  384.1 33.9 %collective-permute-start = (bf16[30,512]{1,0:T(8,128)(2,1)}, bf16[30,512]{1,0:T(8,128)(2,1)}, u32[]{:S(2)}, u32[]{:S(2)}) collective-permute-start(bf16[30,512]{1,0:T(8,128)(2,1)} %slice.256), channel_id=1, source_target_pairs={{0,8},{8,16},{16,24},{1,9},{9,17},{17,25},{2,10},{10,18},{18,26},{... | collective-permute-start | bytes 92168 | tf_op jit(solution)/shard_map/ppermute | solution.py:14
  389.1 25.4 %copy-start.4 = (f32[4,8,64,32]{3,1,2,0:T(8,128)S(1)}, f32[4,8,64,32]{3,1,2,0:T(8,128)}, u32[]{:S(2)}) copy-start(f32[4,8,64,32]{3,1,2,0:T(8,128)} %get-tuple-element.71) | copy-start | bytes 786436
  392.4 22.2 %copy-start.5 = (f32[4,8,32,64]{3,2,1,0:T(8,128)S(1)}, f32[4,8,32,64]{3,2,1,0:T(8,128)}, u32[]{:S(2)}) copy-start(f32[4,8,32,64]{3,2,1,0:T(8,128)} %get-tuple-element.34) | copy-start | bytes 786436
  392.4 22.2 %copy-start.6 = (f32[4,8,32]{2,1,0:T(8,128)S(1)}, f32[4,8,32]{2,1,0:T(8,128)}, u32[]{:S(2)}) copy-start(f32[4,8,32]{2,1,0:T(8,128)} %fusion.26) | copy-start | bytes 12292
  392.4 24.6 %copy-start.41 = (f32[64]{0:T(128)S(1)}, f32[64]{0:T(128)}, u32[]{:S(2)}) copy-start(f32[64]{0:T(128)} %param.35) | copy-start | bytes 772
  416.7 2.1 copy-start.8
  416.7 2.1 copy-start.9
  416.7 2.1 copy-start.10
  416.7 2.1 copy-start.11
  416.7 2.1 copy-start.12
  416.7 2.1 copy-start.13
  416.8 2.1 copy-start.14
  416.8 2.1 copy-start.15
  416.8 2.1 copy-start.16
  416.8 2.1 copy-start.17
  416.8 2.1 copy-start.18
  416.8 2.1 copy-start.19
  416.8 2.1 copy-start.20
  416.8 2.1 copy-start.21
  416.8 2.1 copy-start.22
  416.8 2.1 copy-start.23
  416.9 2.1 copy-start.24
  416.9 2.1 copy-start.25
  416.9 2.1 copy-start.26
  416.9 2.1 copy-start.27
  416.9 2.1 copy-start.28
  416.9 2.1 copy-start.29
  416.9 2.1 copy-start.30
  416.9 2.1 copy-start.31
  416.9 2.1 copy-start.32
  416.9 2.1 copy-start.33
  417.0 2.1 copy-start.34
  417.0 2.1 copy-start.35
  417.0 2.1 copy-start.36
  417.0 2.1 copy-start.37
  417.0 2.1 copy-start.38
  419.1 39.3 %copy-start.7 = (f32[512]{0:T(512)S(1)}, f32[512]{0:T(512)}, u32[]{:S(2)}) copy-start(f32[512]{0:T(512)} %dynamic_slice.28) | copy-start | bytes 6148
  458.4 154.0 %copy-start.40 = (f32[256]{0:T(256)S(1)}, f32[256]{0:T(256)}, u32[]{:S(2)}) copy-start(f32[256]{0:T(256)} %copy-done.39) | copy-start | bytes 3076
  458.4 154.0 %copy-start.46 = (f32[4096]{0:T(1024)S(1)}, f32[4096]{0:T(1024)}, u32[]{:S(2)}) copy-start(f32[4096]{0:T(1024)} %param.20) | copy-start | bytes 49156
  464.0 166.0 %copy-start.2 = (bf16[1,256,2048]{2,1,0:T(8,128)(2,1)S(1)}, bf16[1,256,2048]{2,1,0:T(8,128)(2,1)}, u32[]{:S(2)}) copy-start(bf16[1,256,2048]{2,1,0:T(8,128)(2,1)} %param.19) | copy-start | bytes 3145732
  612.4 20.1 %copy-start.1 = (bf16[4096,64]{0,1:T(8,128)(2,1)S(1)}, bf16[4096,64]{0,1:T(8,128)(2,1)}, u32[]{:S(2)}) copy-start(bf16[4096,64]{0,1:T(8,128)(2,1)} %param.29) | copy-start | bytes 1572868
Sparse Core Ops, SparseCore 0:
  8.9 13.2 all-gather.28
  25.0 61.5 all-gather.20
  89.4 59.1 all-gather.18
  151.2 74.3 all-gather.22
  228.2 74.1 all-gather.14
  305.1 74.1 all-gather.12
  382.1 76.3 all-gather.16
  461.2 74.1 all-gather.24
  538.2 74.1 all-gather.26
  621.7 8.2 reduce-scatter.1
where the time goes:
time: 641 us; the launch traced here: 639 us
  waiting for transfers between devices  429 us (67%)
  other arithmetic  64.9 us (10%)
  local copies, waits for them, and re-layouts  48.8 us (8%)
  matrix products  43.4 us (7%)
  blocking collectives  34.6 us (5%)
  between operations  14.5 us (2%)
    all_gather x1, waiting for transfers between devices, shards(): lax.all_gather(gla_out_w, ('sp', 'fs'), axis=0, tiled=True)  77 us
    all_gather x1, waiting for transfers between devices, shards(): lax.all_gather(conv_in_b, ('sp', 'fs'), axis=0, tiled=True)  72.5 us
    all_gather x1, waiting for transfers between devices, shards(): lax.all_gather(conv_in_a, ('sp', 'fs'), axis=0, tiled=True)  71.9 us
    all_gather x1, waiting for transfers between devices, shards(): lax.all_gather(out_gate_w, ('sp', 'fs'), axis=0, tiled=True)  71.4 us
    all_gather x1, waiting for transfers between devices, shards(): lax.all_gather(value_w, ('sp', 'fs'), axis=0, tiled=True)  55.8 us
    unnamed x95, local copies, waits for them, and re-layouts  35.6 us
    all_gather x1, waiting for transfers between devices, shards(): lax.all_gather(pointwise_w, ('sp', 'fs'), axis=0, tiled=True)  34.2 us
    all_gather x1, waiting for transfers between devices, shards(): lax.all_gather(key_w, ('sp', 'fs'), axis=0, tiled=True)  28.6 us
  transfers between devices with their start and end apart: 11, of which 9 were waited for; matrix products, arithmetic and copies ran while one was open for 23% of the time, Pallas kernels for 0%

commit v1 on v0

--- a/solution.py
+++ b/solution.py
@@ -1,11 +1,204 @@
+import functools
+
 import jax
 import jax.numpy as jnp
 from jax import lax
+from jax.experimental import pallas as pl
+from jax.experimental.pallas import tpu as pltpu
 from jax.sharding import PartitionSpec as P
 
 DK = 32
 DV = 64
+SUB = 16
 BLOCK = 64
+
+
+def gla_kernel(q_ref, k_ref, v_ref, g_ref, ld_ref, hg_ref, o_ref, state_ref, *, rows, chunk):
+    kw = q_ref.shape[1]
+    vw = v_ref.shape[1]
+    f32, bf16 = jnp.float32, jnp.bfloat16
+    spread = (
+        lax.broadcasted_iota(jnp.int32, (kw, vw), 0) // DK
+        == lax.broadcasted_iota(jnp.int32, (kw, vw), 1) // DV
+    ).astype(bf16)
+    own = (
+        lax.broadcasted_iota(jnp.int32, (vw, kw), 1) // DK
+        == lax.broadcasted_iota(jnp.int32, (vw, kw), 0) // DV
+    )
+    head_mean = jnp.where(
+        lax.broadcasted_iota(jnp.int32, (vw, vw), 0) // DV
+        == lax.broadcasted_iota(jnp.int32, (vw, vw), 1) // DV,
+        1.0 / DV,
+        0.0,
+    ).astype(f32)
+    state_ref[...] = jnp.zeros_like(state_ref)
+    place = lax.broadcasted_iota(jnp.int32, (chunk, kw), 0) % SUB
+
+    def body(n, carry):
+        at = pl.ds(pl.multiple_of(n * chunk, chunk), chunk)
+        q = q_ref[at, :].astype(f32) * DK ** (-0.5)
+        k = k_ref[at, :].astype(f32)
+        v = v_ref[at, :].astype(f32)
+        cum = ld_ref[at, :]
+        step = 1
+        while step < SUB:
+            cum = cum + jnp.where(place >= step, pltpu.roll(cum, step, 0), 0.0)
+            step *= 2
+        acc = jnp.dot((q * k).astype(bf16), spread, preferred_element_type=f32) * v
+        for lag in range(1, SUB):
+            decay = jnp.exp(jnp.where(place >= lag, cum - pltpu.roll(cum, lag, 0), -jnp.inf))
+            term = (q * pltpu.roll(k, lag, 0) * decay).astype(bf16)
+            score = jnp.dot(term, spread, preferred_element_type=f32)
+            acc = acc + score * pltpu.roll(v, lag, 0)
+        q_in = (q * jnp.exp(cum)).astype(bf16)
+        v_low = v.astype(bf16)
+        state = state_ref[...]
+        outer = []
+        for m in range(chunk // SUB):
+            part = slice(m * SUB, (m + 1) * SUB)
+            total = cum[(m + 1) * SUB - 1 : (m + 1) * SUB]
+            k_out = (k[part] * jnp.exp(total - cum[part])).astype(bf16)
+            outer.append(
+                lax.dot_general(
+                    q_in[part], state.astype(bf16), (((1,), (1,)), ((), ())),
+                    preferred_element_type=f32,
+                )
+            )
+            added = lax.dot_general(
+                v_low[part], k_out, (((0,), (0,)), ((), ())), preferred_element_type=f32
+            )
+            state = state * jnp.exp(total) + jnp.where(own, added, 0.0)
+        state_ref[...] = state
+        raw = acc + jnp.concatenate(outer, axis=0)
+        mean = jnp.dot(
+            raw * raw, head_mean, preferred_element_type=f32, precision=lax.Precision.HIGHEST
+        )
+        gate = g_ref[at, :].astype(f32)
+        o_ref[at, :] = (
+            raw * lax.rsqrt(mean + 1e-06) * hg_ref[...] * (gate * jax.nn.sigmoid(gate))
+        ).astype(o_ref.dtype)
+        return carry
+
+    lax.fori_loop(0, rows // chunk, body, 0)
+
+
+def gla(queries, keys, values, gate, log_decay, gain):
+    rows, kw = queries.shape
+    vw = values.shape[1]
+    return pl.pallas_call(
+        functools.partial(gla_kernel, rows=rows, chunk=128),
+        out_shape=jax.ShapeDtypeStruct((rows, vw), jnp.bfloat16),
+        in_specs=[pl.BlockSpec(memory_space=pltpu.VMEM)] * 6,
+        out_specs=pl.BlockSpec(memory_space=pltpu.VMEM),
+        scratch_shapes=[pltpu.VMEM((vw, kw), jnp.float32)],
+        cost_estimate=pl.CostEstimate(
+            flops=40_000_000_000, bytes_accessed=4_000_000, transcendentals=2_000_000
+        ),
+        name="gla",
+    )(queries, keys, values, gate, log_decay, gain)
+
+
+def spread_columns(weights, count):
+    return jnp.concatenate(
+        [w.reshape(w.shape[0], count, w.shape[1] // count) for w in weights], axis=2
+    ).transpose(1, 0, 2)
+
+
+def by_heads(
+    inputs,
+    norm_gain,
+    conv_in_a,
+    conv_in_b,
+    query_w,
+    key_w,
+    value_w,
+    out_gate_w,
+    pointwise_w,
+    gla_out_w,
+    forget_first_factor,
+    decay_w,
+    decay_bias,
+    decay_extra,
+    conv_kernel,
+    conv_gain,
+    head_gain,
+):
+    bf16, f32 = jnp.bfloat16, jnp.float32
+    n_sp = lax.axis_size("sp")
+    n_tp = lax.axis_size("tp")
+    n_fs = lax.axis_size("fs")
+    sp, tp = lax.axis_index("sp"), lax.axis_index("tp")
+    tokens = inputs.shape[1]
+    length = n_sp * tokens
+    own_rows = inputs[0]
+    in_weights = (conv_in_a, conv_in_b, query_w, key_w, value_w, out_gate_w)
+    widths = [w.shape[1] // n_sp for w in in_weights]
+    chunks = lax.all_to_all(spread_columns(in_weights, n_sp), "sp", 0, 0)
+    rows = chunks.shape[1]
+    in_full = lax.all_gather(chunks, "fs", axis=1).reshape(n_sp * n_fs * rows, sum(widths))
+    out_local = jnp.concatenate([pointwise_w, gla_out_w], axis=1)
+    out_full = lax.all_gather(out_local, "fs", axis=0, tiled=True)
+    half = lax.all_gather(own_rows, "sp", axis=0, tiled=True)
+    x = lax.all_gather(half, "tp", axis=1, tiled=True)
+    features = x.shape[1]
+    xf = x.astype(f32)
+    row_scale = lax.rsqrt(jnp.sum(xf * xf, axis=1) / features + 1e-06)[:, None]
+    scaled = (xf * norm_gain).astype(bf16)
+
+    product = jnp.dot(scaled, in_full, preferred_element_type=f32)
+    product = (product * row_scale).astype(bf16)
+    at, parts = 0, []
+    for width in widths:
+        parts.append(product[:, at : at + width])
+        at += width
+    conv_a, conv_b, queries, keys, values, out_gate = parts
+    low_rank = (
+        jnp.dot(scaled, forget_first_factor, preferred_element_type=f32) * row_scale
+    ).astype(bf16)
+
+    gated = (conv_a.astype(f32) * jax.nn.sigmoid(conv_b.astype(f32))).astype(bf16)
+    channels = gated.shape[1]
+    taps = conv_kernel.shape[0]
+    first = (tp * n_sp + sp) * channels
+    kernel = lax.dynamic_slice_in_dim(conv_kernel, first, channels, 1)
+    extended = jnp.pad(gated.astype(f32), ((taps - 1, 0), (0, 0)))
+    convolved = jnp.zeros((length, channels), f32)
+    for offset in range(taps):
+        convolved = convolved + kernel[offset] * extended[offset : offset + length]
+    stats = lax.psum(
+        jnp.stack([jnp.sum(convolved, axis=1), jnp.sum(convolved * convolved, axis=1)]),
+        ("sp", "tp"),
+    )
+    total = conv_gain.shape[0]
+    average = stats[0] / total
+    variance = stats[1] / total - average * average
+    gain_part = lax.dynamic_slice_in_dim(conv_gain, first, channels)
+    normed = (convolved - average[:, None]) * lax.rsqrt(variance + 1e-05)[:, None] * gain_part
+    conv_act = jax.nn.silu(normed).astype(bf16)
+
+    key_width = keys.shape[1]
+    first_key = (tp * n_sp + sp) * key_width
+    decay_part = lax.dynamic_slice_in_dim(decay_w, first_key, key_width, 1)
+    bias_part = lax.dynamic_slice_in_dim(decay_bias, first_key, key_width)
+    extra = decay_extra[0].reshape(tokens, n_sp, key_width).transpose(1, 0, 2)
+    extra = lax.all_to_all(extra, "sp", 0, 0).reshape(length, key_width)
+    pre_decay = jnp.dot(low_rank, decay_part, preferred_element_type=f32) + bias_part
+    log_decay = jax.nn.log_sigmoid(pre_decay) / 16.0 + extra
+    gains = jnp.tile(head_gain, key_width // DK)[None]
+    gla_act = gla(queries, keys, values, out_gate, log_decay, gains)
+
+    acts = jnp.stack([conv_act, gla_act])
+    acts = lax.all_gather(acts, "sp", axis=0)
+    acts = acts.transpose(2, 1, 0, 3).reshape(length, 2 * n_sp * channels)
+    partial = lax.dot_general(
+        acts, out_full, (((1,), (1,)), ((), ())), preferred_element_type=f32
+    ).astype(bf16)
+    partial = partial.reshape(n_sp, tokens, partial.shape[1])
+    partial = lax.all_to_all(partial, "sp", 0, 0)
+    partial = partial.reshape(n_tp, n_sp // n_tp, tokens, partial.shape[2])
+    summed = lax.psum_scatter(partial, "tp", scatter_dimension=0, tiled=False)
+    summed = summed.transpose(1, 0, 2).reshape(tokens, own_rows.shape[1])
+    return (own_rows.astype(f32) + summed.astype(f32)).astype(bf16)[None]
 
 
 def from_behind(value, axis, by):
@@ -14,7 +207,7 @@
     return lax.ppermute(value, axis, pairs)
 
 
-def shards(
+def by_tokens(
     inputs,
     norm_gain,
     conv_in_a,
@@ -179,29 +372,21 @@
     return (tok_rows.astype(jnp.float32) + summed.T).astype(jnp.bfloat16)[None]
 
 
+def shards(*args):
+    n_sp, n_tp = lax.axis_size("sp"), lax.axis_size("tp")
+    head_count = args[5].shape[1] // DK
+    whole_heads = head_count % n_sp == 0 and n_sp % n_tp == 0
+    return by_heads(*args) if whole_heads else by_tokens(*args)
+
+
 def solution(mesh):
+    by_rows = P(("sp", "fs"), "tp")
     return jax.shard_map(
         shards,
         mesh=mesh,
-        in_specs=(
-            P("fs", "sp", "tp"),
-            P(),
-            P(("sp", "fs"), "tp"),
-            P(("sp", "fs"), "tp"),
-            P(("sp", "fs"), "tp"),
-            P(("sp", "fs"), "tp"),
-            P(("sp", "fs"), "tp"),
-            P(("sp", "fs"), "tp"),
-            P(("sp", "fs"), "tp"),
-            P(("sp", "fs"), "tp"),
-            P(),
-            P(),
-            P(),
-            P("fs", "sp", "tp"),
-            P(),
-            P(),
-            P(),
-        ),
+        in_specs=(P("fs", "sp", "tp"), P())
+        + (by_rows,) * 8
+        + (P(), P(), P(), P("fs", "sp", "tp"), P(), P(), P()),
         out_specs=P("fs", "sp", "tp"),
         check_vma=False,
     )

time: 641 us -> 414 us (0.65)
  waiting for transfers between devices: 429 us -> 184 us
  blocking collectives: 34.6 us -> 140 us
  other arithmetic: 64.9 us -> 11.4 us
  matrix products: 43.4 us -> 20.4 us
  local copies, waits for them, and re-layouts: 48.8 us -> 26.8 us
  Pallas kernels: 0 us -> 13.3 us
    all_gather x9 -> x5, waiting for transfers between devices: 415 us -> 172 us  [the longest x1 47.6 us: by_heads(): lax.all_gather(chunks, 'fs', axis=1)]
    all_to_all x0 -> x2, blocking collectives: none -> 123 us  [the longest x1 70.3 us: by_heads(): chunks = lax.all_to_all(spread_columns(in_weights, n_sp), 'sp', 0, 0)]
    all_gather x2 -> x0, blocking collectives: 32.1 us -> none  [the longest x1 18.4 us: shards(): piece = lax.all_gather(local_final[None], 'sp', axis=0, tiled=True)]
    unnamed x95 -> x37, local copies, waits for them, and re-layouts: 35.6 us -> 6.74 us
    another operation x3, other arithmetic: 26.6 us -> 2.16 us  [the longest x2 2.15 us: by_heads(): acts = jnp.stack([conv_act, gla_act])]
    dot_general x12 -> x3, matrix products: 43.4 us -> 20.4 us  [the longest x1 9.17 us: by_heads(): product = jnp.dot(scaled, in_full, preferred_element_type=f32)]
    psum x1, blocking collectives: 2.47 us -> 17.5 us  [by_heads(): lax.psum(jnp.stack([jnp.sum(convolved, axis=1), jnp.sum(convolved * convo...]
    pallas_call x0 -> x1, Pallas kernels: none -> 13.3 us  [gla(): pl.pallas_call(functools.partial(gla_kernel, rows=rows, chunk=128), out_s...]
  transfers between devices with their start and end apart: 11 -> 7, of which waited for: 9 -> 7; matrix products, arithmetic and copies ran while one was open for 23% -> 5% of each run, Pallas kernels for 0% -> 0%
where the time goes in v1:
time: 414 us; the launch traced here: 413 us
  waiting for transfers between devices  184 us (44%)
  blocking collectives  140 us (34%)
  local copies, waits for them, and re-layouts  26.8 us (6%)
  matrix products  20.4 us (5%)
  between operations  13.8 us (3%)
  Pallas kernels  13.3 us (3%)
  other arithmetic  11.4 us (3%)
    all_to_all x1, blocking collectives, by_heads(): chunks = lax.all_to_all(spread_columns(in_weights, n_sp), 'sp', 0, 0)  70.3 us
    all_to_all x1, blocking collectives, by_heads(): partial = lax.all_to_all(partial, 'sp', 0, 0)  52.5 us
    all_gather x1, waiting for transfers between devices, by_heads(): lax.all_gather(chunks, 'fs', axis=1)  47.6 us
    all_gather x1, waiting for transfers between devices, by_heads(): acts = lax.all_gather(acts, 'sp', axis=0)  42.9 us
    all_gather x1, waiting for transfers between devices, by_heads(): half = lax.all_gather(own_rows, 'sp', axis=0, tiled=True)  34.9 us
    all_gather x1, waiting for transfers between devices, by_heads(): out_full = lax.all_gather(out_local, 'fs', axis=0, tiled=True)  32.7 us
    psum x1, blocking collectives, by_heads(): lax.psum(jnp.stack([jnp.sum(convolved, axis=1), jnp.sum(convolved * convo...  17.5 us
    all_gather x1, waiting for transfers between devices, by_heads(): x = lax.all_gather(half, 'tp', axis=1, tiled=True)  13.6 us
  transfers between devices with their start and end apart: 7, of which 7 were waited for; matrix products, arithmetic and copies ran while one was open for 5% of the time, Pallas kernels for 0%

profile of v1, /device:TPU:0, one launch (start us, length us, event | category | flops | bytes accessed | tf_op | source)
XLA Modules:
  0.0 413.4 jit_solution(5145605457415467529)
XLA Ops:
  6.5 0.0 copy-start
  6.5 0.0 all-gather.12.cloned.1.call-start
  6.6 0.7 all-gather.12.cloned.1.call-update
  7.3 0.0 all-gather.16.cloned.1.call-start
  7.3 1.1 copy.57
  8.4 1.1 copy.58
  9.5 0.0 copy-done.8
  9.5 0.1 copy.59
  9.6 0.0 copy-done.9
  9.6 0.1 copy.60
  9.7 0.0 copy-done.3
  9.8 0.1 copy.61
  9.9 0.0 copy-done.4
  9.9 0.1 copy.62
  10.2 70.3 %all_to_all.15 = bf16[4,256,640]{1,2,0:T(8,128)(2,1)} all-to-all(bf16[4,256,640]{1,2,0:T(8,128)(2,1)S(1)} %bitcast.124), channel_id=1, replica_groups=mesh['sp'=4,'fs'=4,'tp'=2] {'sp'}, dimensions={0} | all-to-all | bytes 2621440 | tf_op jit(solution)/shard_map/all_to_all | solution.py:136
  80.5 0.0 all-gather.16.cloned.1.call-update
  80.5 0.0 all-gather.14.cloned.1.call-start
  80.6 34.9 %all-gather.12.cloned.1.call-done = bf16[1,1024,2048]{2,1,0:T(8,128)(2,1)} async-done(((bf16[1,256,2048]{2,1,0:T(8,128)(2,1)}), bf16[1,1024,2048]{2,1,0:T(8,128)(2,1)}) %all-gather.12.cloned.1.call-update) | async-done | bytes 4194320 | tf_op jit(solution)/shard_map/all_gather | solution.py:141
  115.5 0.0 all-gather.14.cloned.1.call-update
  115.6 0.9 copy-done.5
  116.5 0.8 copy.66
  117.3 3.4 all-to-all-start.1
  120.7 0.0 all-gather.18.cloned.1.call-start
  120.8 0.0 copy-done.11
  120.8 0.6 broadcast_in_dim_tile.3.hg_ref
  121.4 0.8 dynamic_slice.15
  122.1 0.8 dynamic_slice.13
  122.9 1.1 dynamic-slice_bitcast_fusion.29
  124.0 1.1 dynamic-slice_bitcast_fusion.30
  125.1 4.9 %all-to-all-done.1 = f32[4,256,64]{1,2,0:T(8,128)S(1)} async-done(((f32[4,256,64]{1,2,0:T(8,128)}), f32[4,256,64]{1,2,0:T(8,128)S(1)}, u32[]{:S(2)}, u32[]{:S(2)}) %all-to-all-start.1) | async-done | bytes 262176 | tf_op jit(solution)/shard_map/all_to_all | solution.py:184
  130.0 0.2 copy.67
  130.2 47.6 %all-gather.16.cloned.1.call-done = bf16[4,1024,640]{1,2,0:T(8,128)(2,1)} async-done(((bf16[4,256,640]{1,2,0:T(8,128)(2,1)}), bf16[4,1024,640]{1,2,0:T(8,128)(2,1)}) %all-gather.16.cloned.1.call-update) | async-done | bytes 5242896 | tf_op jit(solution)/shard_map/all_gather | solution.py:138
  177.8 7.9 %copy.63 = bf16[4,1024,640]{2,1,0:T(8,128)(2,1)} copy(bf16[4,1024,640]{1,2,0:T(8,128)(2,1)} %all-gather.16.cloned.1.call-done) | data formatting | bytes 10485760 | tf_op jit(solution)/shard_map/all_gather | solution.py:138
  185.7 13.6 %all-gather.14.cloned.1.call-done = bf16[1,1024,4096]{2,1,0:T(8,128)(2,1)} async-done(((bf16[1,1024,2048]{2,1,0:T(8,128)(2,1)}), bf16[1,1024,4096]{2,1,0:T(8,128)(2,1)}) %all-gather.14.cloned.1.call-update) | async-done | bytes 8388624 | tf_op jit(solution)/shard_map/all_gather | solution.py:142
  199.3 5.2 %fusion.1 = f32[1024]{0:T(1024)S(1)} fusion(bf16[1,1024,4096]{2,1,0:T(8,128)(2,1)} %all-gather.14.cloned.1.call-done), kind=kLoop, calls=%fused_computation.3 | loop fusion | flops 12581888 | bytes 8392704 | tf_op jit(solution)/shard_map/reduce_sum | solution.py:145
  204.5 0.5 copy-done.1
  205.0 9.2 %multiply_convert_fusion = bf16[1024,640]{1,0:T(8,128)(2,1)S(1)} fusion(bf16[4096,640]{1,0:T(8,128)(2,1)} %bitcast.120, bf16[1,1024,4096]{2,1,0:T(8,128)(2,1)S(1)} %copy-done.1, f32[4096]{0:T(1024)S(1)} %copy-done.10, f32[1024]{0:T(1024)S(1)} %add_rsqrt_fusion.1), kind=kOutput, calls=%fused_computation.6 | convolution fusion | flops 5382602752 | bytes 14962688 | tf_op jit(solution)/shard_map/dot_general | solution.py:148
  214.2 1.0 fusion.51
  215.2 0.8 fusion.50
  216.0 0.1 fusion.44
  216.1 2.4 fusion.49
  218.6 17.5 %psum.7 = f32[2,1024]{1,0:T(2,128)S(1)} all-reduce(f32[2,1024]{1,0:T(2,128)S(1)} %pad_maximum_fusion.2), channel_id=1, replica_groups=mesh['sp'=4,'fs'=4,'tp'=2] {'sp','tp'}, use_global_device_ids=true, to_apply=%region_3.4 | all-reduce | flops 2048 | bytes 16384 | tf_op jit(solution)/shard_map/psum | solution.py:168
  236.2 0.4 fusion.45
  236.5 7.2 %fusion.20.ld_ref = f32[1024,64]{1,0:T(8,128)} fusion(f32[4,256,64]{2,1,0:T(8,128)S(1)} %copy.67, bf16[4096,64]{0,1:T(8,128)(2,1)S(1)} %copy-done, bf16[1,1024,4096]{2,1,0:T(8,128)(2,1)} %all-gather.14.cloned.1.call-done, f32[4096]{0:T(1024)S(1)} %copy-done.10, f32[64]{0:T(128)S(1)} %dynamic_slice.15, f32[1024]{0:T(1024)S(1)} %add_rsqrt_fusion.1, ...), kind=kOutput, calls=%fused_computation.18 | convolution fusion | flops 558694400 | bytes 9474308 | tf_op jit(solution)/shard_map/dot_general | solution.py:185
  243.8 13.3 %gla.1 = bf16[1024,128]{1,0:T(8,128)(2,1)} custom-call(bf16[1024,64]{1,0:T(8,128)(2,1)} %get-tuple-element.11.q_ref, bf16[1024,64]{1,0:T(8,128)(2,1)} %get-tuple-element.10.k_ref, bf16[1024,128]{1,0:T(8,128)(2,1)} %get-tuple-element.9.v_ref, bf16[1024,128]{1,0:T(8,128)(2,1)} %get-tuple-element.8.g_ref, f32[1024,64]{1,0:T(8,128)} %fusion.20.ld_ref, ...), custom_call_target="tpu_custom_call" | custom-call | flops 40000000000 | bytes 4000000 | tf_op jit(solution)/shard_map/gla/pallas_call | solution.py:88
  257.1 1.8 pad_maximum_fusion
  258.9 0.0 all-gather.18.cloned.1.call-update
  258.9 0.0 all-gather.10.cloned.1.call-start
  258.9 0.9 pad_maximum_fusion.1
  259.8 0.0 all-gather.10.cloned.1.call-update
  259.8 0.0 reduce-scatter.2.cloned.1.call-start
  259.9 42.9 %all-gather.18.cloned.1.call-done = bf16[8,1024,128]{2,1,0:T(8,128)(2,1)} async-done(((bf16[2,1024,128]{2,1,0:T(8,128)(2,1)}), bf16[8,1024,128]{2,1,0:T(8,128)(2,1)}) %all-gather.18.cloned.1.call-update) | async-done | bytes 2097168 | tf_op jit(solution)/shard_map/all_gather | solution.py:191
  302.8 3.0 copy.68
  305.8 32.7 %all-gather.10.cloned.1.call-done = bf16[1024,1024]{1,0:T(8,128)(2,1)} async-done(((bf16[256,1024]{1,0:T(8,128)(2,1)}), bf16[1024,1024]{1,0:T(8,128)(2,1)}) %all-gather.10.cloned.1.call-update) | async-done | bytes 2097168 | tf_op jit(solution)/shard_map/all_gather | solution.py:140
  338.5 4.0 convolution_convert_fusion
  342.5 52.5 %all_to_all.16 = bf16[4,256,1024]{2,1,0:T(8,128)(2,1)} all-to-all(bf16[4,256,1024]{2,1,0:T(8,128)(2,1)S(1)} %bitcast.123), channel_id=1, replica_groups=mesh['sp'=4,'fs'=4,'tp'=2] {'sp'}, dimensions={0} | all-to-all | bytes 4194304 | tf_op jit(solution)/shard_map/all_to_all | solution.py:197
  395.1 0.0 reduce-scatter.2.cloned.1.call-update
  395.1 1.2 copy-done.2
  396.3 0.5 copy.56
  396.8 6.3 %reduce-scatter.2.cloned.1.call-done = bf16[1,2,256,1024]{3,2,1,0:T(8,128)(2,1)} async-done(((bf16[2,2,256,1024]{3,2,1,0:T(8,128)(2,1)}), bf16[1,2,256,1024]{3,2,1,0:T(8,128)(2,1)}) %reduce-scatter.2.cloned.1.call-update) | async-done | bytes 1048592 | tf_op jit(solution)/shard_map/reduce_scatter | solution.py:199
  403.1 1.5 copy.69
  404.6 0.2 bitcast_convert_fusion
  404.8 0.3 fusion.6
  405.1 1.4 copy.70
  (26 shorter events, 0.2 us)
Async XLA Ops:
  6.5 230.0 %copy-start = (bf16[4096,64]{0,1:T(8,128)(2,1)S(1)}, bf16[4096,64]{0,1:T(8,128)(2,1)}, u32[]{:S(2)}) copy-start(bf16[4096,64]{0,1:T(8,128)(2,1)} %param.27) | copy-start | bytes 1572868
  6.5 3.0 copy-start.8
  6.5 3.1 copy-start.9
  6.5 3.2 copy-start.3
  6.5 3.4 copy-start.4
  6.5 109.0 %all-gather.12.cloned.1.call-start = ((), (), s32[]{:S(2)}) async-start(), calls=%async_computation.6 | async-start | bytes 5242880 | tf_op jit(solution)/shard_map/all_gather | solution.py:141
  7.3 170.5 %all-gather.16.cloned.1.call-start = ((), (), s32[]{:S(2)}) async-start(), calls=%async_computation.8 | async-start | bytes 6553600 | tf_op jit(solution)/shard_map/all_gather | solution.py:138
  80.5 118.7 %all-gather.14.cloned.1.call-start = ((), (), s32[]{:S(2)}) async-start(), calls=%async_computation.7 | async-start | bytes 12582912 | tf_op jit(solution)/shard_map/all_gather | solution.py:142
  115.5 0.9 copy-start.5
  115.5 5.3 %copy-start.11 = (f32[64]{0:T(128)S(1)}, f32[64]{0:T(128)}, u32[]{:S(2)}) copy-start(f32[64]{0:T(128)} %param.33) | copy-start | bytes 772
  117.3 12.7 %all-to-all-start.1 = ((f32[4,256,64]{1,2,0:T(8,128)}), f32[4,256,64]{1,2,0:T(8,128)S(1)}, u32[]{:S(2)}, u32[]{:S(2)}) async-start(f32[4,256,64]{1,2,0:T(8,128)} %bitcast.47), calls=%async_computation.1 | async-start | bytes 524288 | tf_op jit(solution)/shard_map/all_to_all | solution.py:184
  120.7 182.1 %all-gather.18.cloned.1.call-start = ((), (), s32[]{:S(2)}) async-start(), calls=%async_computation.9 | async-start | bytes 2621440 | tf_op jit(solution)/shard_map/all_gather | solution.py:191
  177.8 26.7 %copy-start.10 = (f32[4096]{0:T(1024)S(1)}, f32[4096]{0:T(1024)}, u32[]{:S(2)}) copy-start(f32[4096]{0:T(1024)} %param.18) | copy-start | bytes 49156
  199.3 5.8 %copy-start.1 = (bf16[1,1024,4096]{2,1,0:T(8,128)(2,1)S(1)}, bf16[1,1024,4096]{2,1,0:T(8,128)(2,1)}, u32[]{:S(2)}) copy-start(bf16[1,1024,4096]{2,1,0:T(8,128)(2,1)} %all-gather.14.cloned.1.call-done) | copy-start | bytes 25165828
  243.8 15.2 %copy-start.6 = (bf16[256,512]{1,0:T(8,128)(2,1)S(1)}, bf16[256,512]{1,0:T(8,128)(2,1)}, u32[]{:S(2)}) copy-start(bf16[256,512]{1,0:T(8,128)(2,1)} %param.26) | copy-start | bytes 786436
  243.8 15.2 %copy-start.7 = (bf16[256,512]{1,0:T(8,128)(2,1)S(1)}, bf16[256,512]{1,0:T(8,128)(2,1)}, u32[]{:S(2)}) copy-start(bf16[256,512]{1,0:T(8,128)(2,1)} %param.25) | copy-start | bytes 786436
  258.9 79.7 %all-gather.10.cloned.1.call-start = ((), (), s32[]{:S(2)}) async-start(), calls=%async_computation.4 | async-start | bytes 2621440 | tf_op jit(solution)/shard_map/all_gather | solution.py:140
  259.8 143.3 %reduce-scatter.2.cloned.1.call-start = ((), (), s32[]{:S(2)}) async-start(), calls=%async_computation.5 | async-start | bytes 3145728 | tf_op jit(solution)/shard_map/reduce_scatter | solution.py:199
  395.1 1.2 copy-start.2
Sparse Core Ops, SparseCore 0:
  8.9 106.5 all-gather.11
  117.3 60.4 all-gather.15
  179.4 19.8 all-gather.13
  259.0 43.7 all-gather.17
  304.5 33.9 all-gather.9
  395.2 7.8 reduce-scatter.1
